TPU v7x, 512 devices: a 8x2x16 block of a 8x8x16 slice. The times are simulated.
512 devices in a mesh: grp: 2 (over y), sp: 16 (over z), tp: 16 (over x, core).
Axes of the slice: x: 8, y: 2, z: 16, core: 2. Of those that a mesh axis runs over, the one named last changes fastest.
The devices are a block of a 8x8x16 slice.
Arguments:
- target: bfloat16 [4096, 2048], P(('grp', 'sp', 'tp')), parts along dimension 0, may hold values from -5 to 5
- source: bfloat16 [32768, 2048], P(('grp', 'sp', 'tp')), parts along dimension 0, may hold values from -5 to 5
- source_gain: float32 [2048], replicated, may hold values from 0.1 to 1.9
- pre_first: float32 [2048], replicated, may hold values from 0.1 to 1.9
- query_first: bfloat16 [2048, 2048], P(None, 'tp')
- keyval_first: bfloat16 [2048, 1024], P(None, 'tp')
- out_first: bfloat16 [2048, 2048], P('tp'), may hold values from -0.125 to 0.125
- post_first: float32 [2048], replicated, may hold values from 0.1 to 1.9
- ffn_pre: float32 [2048], replicated, may hold values from 0.1 to 1.9
- w_gate: bfloat16 [2048, 2816], P(None, 'tp'), may hold values from -0.125 to 0.125
- w_value: bfloat16 [2048, 2816], P(None, 'tp'), may hold values from -0.125 to 0.125
- conv_gate: float32 [3, 2816], P(None, 'tp'), may hold values from -3.5 to 3.5
- conv_value: float32 [3, 2816], P(None, 'tp'), may hold values from -3.5 to 3.5
- w_down: bfloat16 [2816, 2048], P('tp'), may hold values from -0.109375 to 0.109375
- ffn_post: float32 [2048], replicated, may hold values from 0.1 to 1.9
- pre_second: float32 [2048], replicated, may hold values from 0.1 to 1.9
- query_second: bfloat16 [2048, 2048], P(None, 'tp')
- keyval_second: bfloat16 [2048, 1024], P(None, 'tp')
- out_second: bfloat16 [2048, 2048], P('tp'), may hold values from -0.125 to 0.125
- post_second: float32 [2048], replicated, may hold values from 0.1 to 1.9
Outputs:
- decoded: float32 [4096, 2048], P(('grp', 'sp', 'tp')), parts along dimension 0
There are 2 independent parts, one for each index of `grp`. A program takes and returns all parts, laid end to end along the dimension named above; an argument that names none is the same for every part. Nothing has to cross between parts.
All inputs are finite; a program needn't handle non-finite values.
Results may differ from a plain program's by a relative error of at most 0.04.
Values may be sent and summed in bfloat16 or wider, within the bound.
A program may use at most 128 MiB of HBM per device.

v0:
```python
import jax
import jax.numpy as jnp
from jax import lax
from jax.sharding import PartitionSpec as P

HEAD = 128
KVH = 4


def in_blocks(array, dim, size):
    before, after = (array.shape[:dim], array.shape[dim + 1 :])
    return jnp.moveaxis(array.reshape(*before, size, -1, *after), dim, 0)


def sent_and_summed(array, axis, dim):
    parts = in_blocks(array, dim, lax.axis_size(axis))
    arrived = lax.all_to_all(parts, axis, split_axis=0, concat_axis=0, tiled=True)
    return arrived.astype(jnp.float32).sum(axis=0)


def swapped(block, axis, distance):
    count = lax.axis_size(axis)
    route = []
    for low in range(count):
        high = low | 1 << distance
        if high != low and high < count:
            route += [(low, high), (high, low)]
    return lax.ppermute(block, axis, route)


def in_one_piece(arrays, axis, dim, along):
    both = jnp.concatenate(arrays, axis=along)
    result, at, done = (lax.all_gather(both, axis, axis=dim, tiled=True), 0, [])
    for a in arrays:
        done.append(lax.slice_in_dim(result, at, at + a.shape[along], axis=along))
        at += a.shape[along]
    return tuple(done)


def shifted(value, axis, steps):
    count = lax.axis_size(axis)
    leading, last = (max(0, -steps), min(count, count - steps))
    return lax.ppermute(value, axis, [(source, source + steps) for source in range(leading, last)])


def normed(values, gain):
    widened = values.astype(jnp.float32)
    return widened * lax.rsqrt(jnp.mean(widened * widened, axis=-1, keepdims=True) + 1e-06) * gain


def project_rows(rows_here, weights):
    shard_rows = lax.all_gather(rows_here, "tp", axis=0, tiled=True)
    products = [
        jnp.dot(shard_rows, weight, preferred_element_type=jnp.float32).astype(jnp.bfloat16)
        for weight in weights
    ]
    return jnp.concatenate(products, axis=1)


def summed_rows(parts, weight):
    return sent_and_summed(
        jnp.dot(parts, weight, preferred_element_type=jnp.float32).astype(jnp.bfloat16), "tp", 0
    )


def key_columns(source_rows, keyval_first, keyval_second):
    both_layers = jnp.concatenate([keyval_first, keyval_second], axis=1)
    columns = jnp.einsum(
        "rd,dc->cr",
        lax.all_gather(source_rows, "tp", axis=0, tiled=True),
        both_layers,
        preferred_element_type=jnp.float32,
    ).astype(jnp.bfloat16)
    column_count = keyval_first.shape[1]
    stacked = columns.reshape(2, column_count, columns.shape[1])
    own_index = lax.axis_index("tp")
    doublings = (2 * HEAD // column_count).bit_length() - 1
    for bit_number in range(doublings):
        lower_half = own_index // 2**bit_number % 2 == 0
        half_rows = stacked.shape[2] // 2
        outgoing = jnp.where(lower_half, stacked[:, :, half_rows:], stacked[:, :, :half_rows])
        retained = jnp.where(lower_half, stacked[:, :, :half_rows], stacked[:, :, half_rows:])
        partner = swapped(outgoing, "tp", bit_number)
        stacked = jnp.where(
            lower_half,
            jnp.concatenate([retained, partner], axis=1),
            jnp.concatenate([partner, retained], axis=1),
        )
    return (stacked[:, :HEAD], stacked[:, HEAD:])


def absorber(query_heads, running, shard_pair):
    scale_factor = HEAD ** (-0.5)
    best_score, weight_sum, weighted = running
    key_block, value_block = shard_pair
    scores = (
        jnp.einsum("thd,ds->ths", query_heads, key_block, preferred_element_type=jnp.float32)
        * scale_factor
    )
    newest = jnp.max(scores, axis=2)
    rescale = jnp.exp(best_score - newest)
    weights = jnp.exp(scores - newest[:, :, None])
    weight_sum = weight_sum * rescale + jnp.sum(weights, axis=2)
    weighted = weighted * rescale[:, :, None] + jnp.einsum(
        "ths,ds->thd", weights.astype(jnp.bfloat16), value_block, preferred_element_type=jnp.float32
    )
    return (newest, weight_sum, weighted)


def empty_running(row_count, head_count):
    return (
        jnp.full((row_count, head_count), -jnp.inf, jnp.float32),
        jnp.zeros((row_count, head_count), jnp.float32),
        jnp.zeros((row_count, head_count, HEAD), jnp.float32),
    )


def attend_shares(queries, keys_t, values_t):
    row_count = queries.shape[0]
    own_heads = queries.shape[1] // HEAD
    group_count = lax.axis_size("tp") // KVH
    doublings = group_count.bit_length() - 1
    own_index = lax.axis_index("tp")
    grouped = queries
    for bit_number in range(doublings):
        lower_half = own_index // 2**bit_number % 2 == 0
        partner = swapped(grouped, "tp", bit_number)
        grouped = jnp.where(
            lower_half,
            jnp.concatenate([grouped, partner], axis=1),
            jnp.concatenate([partner, grouped], axis=1),
        )
    head_count = grouped.shape[1] // HEAD
    query_heads = grouped.reshape(row_count, head_count, HEAD)
    best_score, weight_sum, weighted = absorber(
        query_heads,
        empty_running(row_count, head_count),
        in_one_piece((keys_t, values_t), "sp", 1, 0),
    )
    for bit_number in range(doublings):
        other_best, other_sum, other_weighted = (
            swapped(best_score.astype(jnp.bfloat16), "tp", bit_number).astype(best_score.dtype),
            swapped(weight_sum.astype(jnp.bfloat16), "tp", bit_number).astype(weight_sum.dtype),
            swapped(weighted.astype(jnp.bfloat16), "tp", bit_number).astype(weighted.dtype),
        )
        newest = jnp.maximum(best_score, other_best)
        own_scale = jnp.exp(best_score - newest)
        other_scale = jnp.exp(other_best - newest)
        weight_sum = weight_sum * own_scale + other_sum * other_scale
        weighted = weighted * own_scale[:, :, None] + other_weighted * other_scale[:, :, None]
        best_score = newest
    first_head = own_index % group_count * own_heads
    chosen = lax.dynamic_slice_in_dim(weighted, first_head, own_heads, 1)
    chosen_sums = lax.dynamic_slice_in_dim(weight_sum, first_head, own_heads, 1)
    return (
        (chosen / chosen_sums[:, :, None]).reshape(row_count, own_heads * HEAD).astype(jnp.bfloat16)
    )


def causal_mix(rim_rows, up_rows, conv_taps):
    padded = jnp.concatenate([rim_rows, up_rows], axis=0).astype(jnp.float32)
    length = up_rows.shape[0]
    return (
        conv_taps[0] * padded[:length]
        + conv_taps[1] * padded[1 : length + 1]
        + conv_taps[2] * padded[2:]
    )


def per_device(
    target,
    source,
    source_gain,
    pre_first,
    query_first,
    keyval_first,
    out_first,
    post_first,
    ffn_pre,
    w_gate,
    w_value,
    conv_gate,
    conv_value,
    w_down,
    ffn_post,
    pre_second,
    query_second,
    keyval_second,
    out_second,
    post_second,
):
    source_rows = normed(source, source_gain).astype(jnp.bfloat16)
    keys_t, values_t = key_columns(source_rows, keyval_first, keyval_second)

    def attention_layer(stream, pre_gain, w_query, layer_index, w_out, post_gain):
        queries = project_rows(normed(stream, pre_gain).astype(jnp.bfloat16), (w_query,))
        heads = attend_shares(queries, keys_t[layer_index], values_t[layer_index])
        mixed = summed_rows(heads, w_out)
        return stream.astype(jnp.float32) + normed(mixed, post_gain)

    after_first = attention_layer(target, pre_first, query_first, 0, out_first, post_first)
    up_both = project_rows(normed(after_first, ffn_pre).astype(jnp.bfloat16), (w_gate, w_value))
    hidden_width = w_gate.shape[1]
    up_gate = up_both[:, :hidden_width]
    up_value = up_both[:, hidden_width:]
    rim_gate, rim_value = shifted((up_gate[-2:], up_value[-2:]), "sp", 1)
    gated = (
        jax.nn.gelu(causal_mix(rim_gate, up_gate, conv_gate), approximate=True)
        * causal_mix(rim_value, up_value, conv_value)
    ).astype(jnp.bfloat16)
    ffn_sum = summed_rows(gated, w_down)
    after_ffn = after_first + normed(ffn_sum, ffn_post)
    return attention_layer(after_ffn, pre_second, query_second, 1, out_second, post_second)


def solution(mesh):
    placed = (
        P(("grp", "sp", "tp"), None),
        P(("grp", "sp", "tp"), None),
        P(),
        P(),
        P(None, "tp"),
        P(None, "tp"),
        P("tp", None),
        P(),
        P(),
        P(None, "tp"),
        P(None, "tp"),
        P(None, "tp"),
        P(None, "tp"),
        P("tp", None),
        P(),
        P(),
        P(None, "tp"),
        P(None, "tp"),
        P("tp", None),
        P(),
    )
    return jax.shard_map(
        per_device,
        mesh=mesh,
        in_specs=placed,
        out_specs=P(("grp", "sp", "tp"), None),
        check_vma=False,
    )
```

profile of v0, /device:TPU:65, one launch (start us, length us, event | category | flops | bytes accessed | tf_op | source)
XLA Modules:
  0.0 380.8 jit_solution(5917875736320434852)
XLA Ops:
  9.8 83.2 %all-gather.4.cloned.1.call-done = bf16[1024,2048]{1,0:T(8,128)(2,1)} async-done(((bf16[64,2048]{1,0:T(8,128)(2,1)}), bf16[1024,2048]{1,0:T(8,128)(2,1)}) %all-gather.4.cloned.1.call-update) | async-done | bytes 4194320 | tf_op jit(solution)/shard_map/all_gather | solution.py:70
  93.0 3.9 %convolution_convert_fusion.3 = bf16[128,1024]{1,0:T(8,128)(2,1)S(1)} fusion(bf16[1024,2048]{1,0:T(8,128)(2,1)} %all-gather.4.cloned.1.call-done, bf16[2048,64]{0,1:T(8,128)(2,1)} %param.37, bf16[2048,64]{0,1:T(8,128)(2,1)} %param.25), kind=kOutput, calls=%fused_computation.16 | convolution fusion | flops 538050560 | bytes 4980736 | tf_op jit(solution)/shard_map/rd,dc->cr/dot_general | solution.py:68
  100.2 3.0 collective-permute-start.3
  103.3 3.7 collective-permute-done.3
  108.7 18.7 %all_gather.18 = bf16[128,2048]{1,0:T(8,128)(2,1)S(1)} all-gather(bf16[8,2048]{1,0:T(8,128)(2,1)S(1)} %fusion.52), channel_id=1, replica_groups=mesh['grp'=2,'sp'=16,'tp'=16] {'tp'}, dimensions={0}, use_global_device_ids=true | all-gather | bytes 557056 | tf_op jit(solution)/shard_map/all_gather | solution.py:52
  132.8 3.5 collective-permute-done.1
  136.4 41.9 %all-gather.6.cloned.1.call-done = bf16[256,4096]{1,0:T(8,128)(2,1)} async-done(((bf16[256,256]{1,0:T(8,128)(2,1)}), bf16[256,4096]{1,0:T(8,128)(2,1)}) %all-gather.6.cloned.1.call-update) | async-done | bytes 2097168 | tf_op jit(solution)/shard_map/all_gather | solution.py:33
  182.7 13.7 %collective-permute-start.4 = (bf16[128,4]{0,1:T(4,128)(2,1)S(1)}, bf16[128,4]{0,1:T(4,128)(2,1)S(1)}, u32[]{:S(2)}, u32[]{:S(2)}) collective-permute-start(bf16[128,4]{0,1:T(4,128)(2,1)S(1)} %get-tuple-element.43), channel_id=1, source_target_pairs={{0,1},{1,0},{2,3},{3,2},{4,5},{5,4},{6,7},{7,6},{8,9},{9,8},{10,11... | collective-permute-start | bytes 3080 | tf_op jit(solution)/shard_map/ppermute | solution.py:28
  198.4 3.5 collective-permute-start.6
  209.2 4.0 %collective-permute-start.5 = (bf16[128,4,128]{2,0,1:T(8,128)(2,1)}, bf16[128,4,128]{2,0,1:T(8,128)(2,1)}, u32[]{:S(2)}, u32[]{:S(2)}) collective-permute-start(bf16[128,4,128]{2,0,1:T(8,128)(2,1)} %get-tuple-element.47), channel_id=1, source_target_pairs={{0,1},{1,0},{2,3},{3,2},{4,5},{5,4},{6,7},{7,6},{8,9},{9,8},{10,11... | collective-permute-start | bytes 393224 | tf_op jit(solution)/shard_map/ppermute | solution.py:28
  218.2 4.0 %collective-permute-done.7 = bf16[128,4,128]{2,0,1:T(8,128)(2,1)S(1)} collective-permute-done((bf16[128,4,128]{2,0,1:T(8,128)(2,1)S(1)}, bf16[128,4,128]{2,0,1:T(8,128)(2,1)S(1)}, u32[]{:S(2)}, u32[]{:S(2)}) %collective-permute-start.7) | collective-permute-done | bytes 131104 | tf_op jit(solution)/shard_map/ppermute | solution.py:28
  223.4 6.5 %all-to-all-start = ((bf16[16,8,2048]{2,1,0:T(8,128)(2,1)}), bf16[16,8,2048]{2,1,0:T(8,128)(2,1)S(1)}, u32[]{:S(2)}, u32[]{:S(2)}) async-start(bf16[16,8,2048]{2,1,0:T(8,128)(2,1)} %fusion.8), calls=%async_computation | async-start | bytes 1048576 | tf_op jit(solution)/shard_map/all_to_all | solution.py:17
  233.2 13.9 %all-to-all-done = bf16[16,8,2048]{2,1,0:T(8,128)(2,1)S(1)} async-done(((bf16[16,8,2048]{2,1,0:T(8,128)(2,1)}), bf16[16,8,2048]{2,1,0:T(8,128)(2,1)S(1)}, u32[]{:S(2)}, u32[]{:S(2)}) %all-to-all-start) | async-done | bytes 524320 | tf_op jit(solution)/shard_map/all_to_all | solution.py:17
  247.6 16.0 %all_gather.21 = bf16[128,2048]{1,0:T(8,128)(2,1)S(1)} all-gather(bf16[8,2048]{1,0:T(8,128)(2,1)S(1)} %multiply_convert_fusion.1), channel_id=1, replica_groups=mesh['grp'=2,'sp'=16,'tp'=16] {'tp'}, dimensions={0}, use_global_device_ids=true | all-gather | bytes 557056 | tf_op jit(solution)/shard_map/all_gather | solution.py:52
  264.1 3.2 collective-permute-start.10
  271.7 23.3 %all_to_all.15 = bf16[16,8,2048]{2,1,0:T(8,128)(2,1)S(1)} all-to-all(bf16[16,8,2048]{2,1,0:T(8,128)(2,1)S(1)} %fusion.9), channel_id=1, replica_groups=mesh['grp'=2,'sp'=16,'tp'=16] {'tp'}, dimensions={0} | all-to-all | bytes 1048576 | tf_op jit(solution)/shard_map/all_to_all | solution.py:17
  295.6 16.0 %all_gather.22 = bf16[128,2048]{1,0:T(8,128)(2,1)S(1)} all-gather(bf16[8,2048]{1,0:T(8,128)(2,1)S(1)} %multiply_convert_fusion), channel_id=1, replica_groups=mesh['grp'=2,'sp'=16,'tp'=16] {'tp'}, dimensions={0}, use_global_device_ids=true | all-gather | bytes 557056 | tf_op jit(solution)/shard_map/all_gather | solution.py:52
  317.3 3.2 collective-permute-done.13
  324.7 3.0 collective-permute-start.14
  331.9 3.2 collective-permute-start.19
  338.0 3.9 %collective-permute-start.15 = (bf16[128,4,128]{2,0,1:T(8,128)(2,1)S(1)}, bf16[128,4,128]{2,0,1:T(8,128)(2,1)S(1)}, u32[]{:S(2)}, u32[]{:S(2)}) collective-permute-start(bf16[128,4,128]{2,0,1:T(8,128)(2,1)S(1)} %get-tuple-element.51), channel_id=1, source_target_pairs={{0,1},{1,0},{2,3},{3,2},{4,5},{5,4},{6,7},{7,6},{8,9},{9,8},{10,11... | collective-permute-start | bytes 393224 | tf_op jit(solution)/shard_map/ppermute | solution.py:28
  343.0 3.2 collective-permute-start.17
  346.2 3.4 collective-permute-done.17
  350.0 23.3 %all_to_all.16 = bf16[16,8,2048]{2,1,0:T(8,128)(2,1)S(1)} all-to-all(bf16[16,8,2048]{2,1,0:T(8,128)(2,1)S(1)} %fusion.10), channel_id=1, replica_groups=mesh['grp'=2,'sp'=16,'tp'=16] {'tp'}, dimensions={0} | all-to-all | bytes 1048576 | tf_op jit(solution)/shard_map/all_to_all | solution.py:17
  (132 shorter events, 62.0 us)
Async XLA Ops:
  6.6 86.4 %all-gather.4.cloned.1.call-start = ((), (), s32[]{:S(2)}) async-start(), calls=%async_computation.3 | async-start | bytes 4456448 | tf_op jit(solution)/shard_map/all_gather | solution.py:70
  9.7 168.6 %all-gather.6.cloned.1.call-start = ((), (), s32[]{:S(2)}) async-start(), calls=%async_computation.4 | async-start | bytes 2228224 | tf_op jit(solution)/shard_map/all_gather | solution.py:33
  96.9 3.3 collective-permute-start.2
  100.2 6.7 %collective-permute-start.3 = (bf16[2,128,256]{2,1,0:T(8,128)(2,1)S(1)}, bf16[2,128,256]{2,1,0:T(8,128)(2,1)S(1)}, u32[]{:S(2)}, u32[]{:S(2)}) collective-permute-start(bf16[2,128,256]{2,1,0:T(8,128)(2,1)S(1)} %get-tuple-element.30), channel_id=1, source_target_pairs={{0,2},{2,0},{1,3},{3,1},{4,6},{6,4},{5,7},{7,5},{8,10},{10,8},{9,1... | collective-permute-start | bytes 393224 | tf_op jit(solution)/shard_map/ppermute | solution.py:28
  127.7 3.1 collective-permute-start
  130.9 5.5 %collective-permute-start.1 = (bf16[128,256]{0,1:T(8,128)(2,1)S(1)}, bf16[128,256]{0,1:T(8,128)(2,1)S(1)}, u32[]{:S(2)}, u32[]{:S(2)}) collective-permute-start(bf16[128,256]{0,1:T(8,128)(2,1)S(1)} %maximum_select_fusion.7), channel_id=1, source_target_pairs={{0,2},{2,0},{1,3},{3,1},{4,6},{6,4},{5,7},{7,5},{8,10},{10,8},{9,1... | collective-permute-start | bytes 196616 | tf_op jit(solution)/shard_map/ppermute | solution.py:28
  182.7 15.7 %collective-permute-start.4 = (bf16[128,4]{0,1:T(4,128)(2,1)S(1)}, bf16[128,4]{0,1:T(4,128)(2,1)S(1)}, u32[]{:S(2)}, u32[]{:S(2)}) collective-permute-start(bf16[128,4]{0,1:T(4,128)(2,1)S(1)} %get-tuple-element.43), channel_id=1, source_target_pairs={{0,1},{1,0},{2,3},{3,2},{4,5},{5,4},{6,7},{7,6},{8,9},{9,8},{10,11... | collective-permute-start | bytes 3080 | tf_op jit(solution)/shard_map/ppermute | solution.py:28
  196.4 5.5 %collective-permute-start.8 = (bf16[128,4]{0,1:T(4,128)(2,1)S(1)}, bf16[128,4]{0,1:T(4,128)(2,1)S(1)}, u32[]{:S(2)}, u32[]{:S(2)}) collective-permute-start(bf16[128,4]{0,1:T(4,128)(2,1)S(1)} %get-tuple-element.44), channel_id=1, source_target_pairs={{0,1},{1,0},{2,3},{3,2},{4,5},{5,4},{6,7},{7,6},{8,9},{9,8},{10,11... | collective-permute-start | bytes 3080 | tf_op jit(solution)/shard_map/ppermute | solution.py:28
  198.4 5.5 %collective-permute-start.6 = (bf16[128,4]{0,1:T(4,128)(2,1)S(1)}, bf16[128,4]{0,1:T(4,128)(2,1)S(1)}, u32[]{:S(2)}, u32[]{:S(2)}) collective-permute-start(bf16[128,4]{0,1:T(4,128)(2,1)S(1)} %fusion.82), channel_id=1, source_target_pairs={{0,2},{2,0},{1,3},{3,1},{4,6},{6,4},{5,7},{7,5},{8,10},{10,8},{9,1... | collective-permute-start | bytes 3080 | tf_op jit(solution)/shard_map/ppermute | solution.py:28
  201.9 4.3 %collective-permute-start.9 = (bf16[128,4]{0,1:T(4,128)(2,1)S(1)}, bf16[128,4]{0,1:T(4,128)(2,1)S(1)}, u32[]{:S(2)}, u32[]{:S(2)}) collective-permute-start(bf16[128,4]{0,1:T(4,128)(2,1)S(1)} %get-tuple-element.19), channel_id=1, source_target_pairs={{0,2},{2,0},{1,3},{3,1},{4,6},{6,4},{5,7},{7,5},{8,10},{10,8},{9,1... | collective-permute-start | bytes 3080 | tf_op jit(solution)/shard_map/ppermute | solution.py:28
  209.2 5.3 %collective-permute-start.5 = (bf16[128,4,128]{2,0,1:T(8,128)(2,1)}, bf16[128,4,128]{2,0,1:T(8,128)(2,1)}, u32[]{:S(2)}, u32[]{:S(2)}) collective-permute-start(bf16[128,4,128]{2,0,1:T(8,128)(2,1)} %get-tuple-element.47), channel_id=1, source_target_pairs={{0,1},{1,0},{2,3},{3,2},{4,5},{5,4},{6,7},{7,6},{8,9},{9,8},{10,11... | collective-permute-start | bytes 393224 | tf_op jit(solution)/shard_map/ppermute | solution.py:28
  215.6 6.6 %collective-permute-start.7 = (bf16[128,4,128]{2,0,1:T(8,128)(2,1)S(1)}, bf16[128,4,128]{2,0,1:T(8,128)(2,1)S(1)}, u32[]{:S(2)}, u32[]{:S(2)}) collective-permute-start(bf16[128,4,128]{2,0,1:T(8,128)(2,1)S(1)} %get-tuple-element.23), channel_id=1, source_target_pairs={{0,2},{2,0},{1,3},{3,1},{4,6},{6,4},{5,7},{7,5},{8,10},{10,8},{9,1... | collective-permute-start | bytes 393224 | tf_op jit(solution)/shard_map/ppermute | solution.py:28
  223.4 23.7 %all-to-all-start = ((bf16[16,8,2048]{2,1,0:T(8,128)(2,1)}), bf16[16,8,2048]{2,1,0:T(8,128)(2,1)S(1)}, u32[]{:S(2)}, u32[]{:S(2)}) async-start(bf16[16,8,2048]{2,1,0:T(8,128)(2,1)} %fusion.8), calls=%async_computation | async-start | bytes 1048576 | tf_op jit(solution)/shard_map/all_to_all | solution.py:17
  229.9 87.4 %all-gather.8.cloned.1.call-start = ((), (), s32[]{:S(2)}) async-start(), calls=%async_computation.5 | async-start | bytes 2228224 | tf_op jit(solution)/shard_map/all_gather | solution.py:33
  264.1 5.8 %collective-permute-start.10 = (bf16[2,176]{0,1:T(8,128)(2,1)S(1)}, bf16[2,176]{0,1:T(8,128)(2,1)S(1)}, u32[]{:S(2)}, u32[]{:S(2)}) collective-permute-start(bf16[2,176]{0,1:T(8,128)(2,1)S(1)} %slice.122), channel_id=1, source_target_pairs={{0,16},{16,32},{32,48},{48,64},{64,80},{80,96},{96,112},{112,128},... | collective-permute-start | bytes 2120 | tf_op jit(solution)/shard_map/ppermute | solution.py:43
  267.8 3.2 collective-permute-start.11
  311.9 3.1 collective-permute-start.12
  315.1 5.4 %collective-permute-start.13 = (bf16[128,256]{0,1:T(8,128)(2,1)S(1)}, bf16[128,256]{0,1:T(8,128)(2,1)S(1)}, u32[]{:S(2)}, u32[]{:S(2)}) collective-permute-start(bf16[128,256]{0,1:T(8,128)(2,1)S(1)} %maximum_select_fusion.9), channel_id=1, source_target_pairs={{0,2},{2,0},{1,3},{3,1},{4,6},{6,4},{5,7},{7,5},{8,10},{10,8},{9,1... | collective-permute-start | bytes 196616 | tf_op jit(solution)/shard_map/ppermute | solution.py:28
  324.7 4.9 %collective-permute-start.14 = (bf16[128,4]{0,1:T(4,128)(2,1)S(1)}, bf16[128,4]{0,1:T(4,128)(2,1)S(1)}, u32[]{:S(2)}, u32[]{:S(2)}) collective-permute-start(bf16[128,4]{0,1:T(4,128)(2,1)S(1)} %get-tuple-element.40), channel_id=1, source_target_pairs={{0,1},{1,0},{2,3},{3,2},{4,5},{5,4},{6,7},{7,6},{8,9},{9,8},{10,11... | collective-permute-start | bytes 3080 | tf_op jit(solution)/shard_map/ppermute | solution.py:28
  327.7 4.2 %collective-permute-start.18 = (bf16[128,4]{0,1:T(4,128)(2,1)S(1)}, bf16[128,4]{0,1:T(4,128)(2,1)S(1)}, u32[]{:S(2)}, u32[]{:S(2)}) collective-permute-start(bf16[128,4]{0,1:T(4,128)(2,1)S(1)} %get-tuple-element.41), channel_id=1, source_target_pairs={{0,1},{1,0},{2,3},{3,2},{4,5},{5,4},{6,7},{7,6},{8,9},{9,8},{10,11... | collective-permute-start | bytes 3080 | tf_op jit(solution)/shard_map/ppermute | solution.py:28
  329.7 5.4 %collective-permute-start.16 = (bf16[128,4]{0,1:T(4,128)(2,1)S(1)}, bf16[128,4]{0,1:T(4,128)(2,1)S(1)}, u32[]{:S(2)}, u32[]{:S(2)}) collective-permute-start(bf16[128,4]{0,1:T(4,128)(2,1)S(1)} %fusion.83), channel_id=1, source_target_pairs={{0,2},{2,0},{1,3},{3,1},{4,6},{6,4},{5,7},{7,5},{8,10},{10,8},{9,1... | collective-permute-start | bytes 3080 | tf_op jit(solution)/shard_map/ppermute | solution.py:28
  331.9 4.3 %collective-permute-start.19 = (bf16[128,4]{0,1:T(4,128)(2,1)S(1)}, bf16[128,4]{0,1:T(4,128)(2,1)S(1)}, u32[]{:S(2)}, u32[]{:S(2)}) collective-permute-start(bf16[128,4]{0,1:T(4,128)(2,1)S(1)} %get-tuple-element.8), channel_id=1, source_target_pairs={{0,2},{2,0},{1,3},{3,1},{4,6},{6,4},{5,7},{7,5},{8,10},{10,8},{9,1... | collective-permute-start | bytes 3080 | tf_op jit(solution)/shard_map/ppermute | solution.py:28
  338.0 4.8 %collective-permute-start.15 = (bf16[128,4,128]{2,0,1:T(8,128)(2,1)S(1)}, bf16[128,4,128]{2,0,1:T(8,128)(2,1)S(1)}, u32[]{:S(2)}, u32[]{:S(2)}) collective-permute-start(bf16[128,4,128]{2,0,1:T(8,128)(2,1)S(1)} %get-tuple-element.51), channel_id=1, source_target_pairs={{0,1},{1,0},{2,3},{3,2},{4,5},{5,4},{6,7},{7,6},{8,9},{9,8},{10,11... | collective-permute-start | bytes 393224 | tf_op jit(solution)/shard_map/ppermute | solution.py:28
  343.0 6.6 %collective-permute-start.17 = (bf16[128,4,128]{2,0,1:T(8,128)(2,1)S(1)}, bf16[128,4,128]{2,0,1:T(8,128)(2,1)S(1)}, u32[]{:S(2)}, u32[]{:S(2)}) collective-permute-start(bf16[128,4,128]{2,0,1:T(8,128)(2,1)S(1)} %get-tuple-element.12), channel_id=1, source_target_pairs={{0,2},{2,0},{1,3},{3,1},{4,6},{6,4},{5,7},{7,5},{8,10},{10,8},{9,1... | collective-permute-start | bytes 393224 | tf_op jit(solution)/shard_map/ppermute | solution.py:28
  (16 other events, 1324.8 us)
Sparse Core Ops, SparseCore 0:
  9.8 83.0 all-gather.3
  108.6 69.7 all-gather.5
  233.3 66.6 all-gather.7
where the time goes:
time: 382 us; the launch traced here: 381 us
  waiting for transfers between devices  167 us (44%)
  blocking collectives  97.2 us (25%)
  starting transfers between devices  70 us (18%)
  matrix products  16.9 us (4%)
  between operations  13.8 us (4%)
  other arithmetic  12.8 us (3%)
    all_gather x1, waiting for transfers between devices, key_columns(): lax.all_gather(source_rows, 'tp', axis=0, tiled=True)  83.2 us
    ppermute x18, starting transfers between devices, swapped(): return lax.ppermute(block, axis, route)  57.9 us
    all_gather x3, blocking collectives, project_rows(): shard_rows = lax.all_gather(rows_here, 'tp', axis=0, tiled=True)  50.6 us
    all_to_all x2, blocking collectives, sent_and_summed(): lax.all_to_all(parts, axis, split_axis=0, concat_axis=0, tiled=True)  46.6 us
    all_gather x2, waiting for transfers between devices, in_one_piece(): result, at, done = (lax.all_gather(both, axis, axis=dim, tiled=True), 0, [])  42 us
    ppermute x18, waiting for transfers between devices, swapped(): return lax.ppermute(block, axis, route)  26.6 us
    all_to_all x1, waiting for transfers between devices, sent_and_summed(): lax.all_to_all(parts, axis, split_axis=0, concat_axis=0, tiled=True)  13.9 us
  transfers between devices with their start and end apart: 24, of which 16 were waited for; matrix products, arithmetic and copies ran while one was open for 2% of the time, Pallas kernels for 0%

commit v1 on v0

v1 whole, which is shorter than its diff:
```python
import functools
import math

import jax
import jax.numpy as jnp
from jax import lax
from jax.experimental import pallas as pl
from jax.experimental.pallas import tpu as pltpu
from jax.sharding import PartitionSpec as P

HEAD = 128
KVH = 4
CORES = 2
SUBS = 4
MESH = pl.DeviceIdType.MESH
F32 = jnp.float32
BF16 = jnp.bfloat16


def normed(v, gain):
    return v * lax.rsqrt(jnp.mean(v * v, axis=-1, keepdims=True) + 1e-6) * gain


def dot(a, b, contract=((1,), (0,))):
    return lax.dot_general(a, b, (contract, ((), ())), preferred_element_type=F32)


def kernel(
    nx, nz,
    tgt_hbm, src_hbm, taps_hbm, sgain, pre1, post1, fpre, fpost, pre2, post2,
    q1_hbm, q2_hbm, kv1_hbm, kv2_hbm, o1_hbm, o2_hbm, wg_hbm, wv_hbm, wd_hbm,
    out_ref,
    src_v, tgt_v, kvin, w2, wq, wo, wgv, wdn, taps,
    rows_x, kv_st, kvb, hb, sb, rb, qb, o_st, ob, s_st, st, acc, m_run, l_run, up, rim, resid,
    loc_sem, w_send, w_recv, x_send, x_recv, e_send, e_recv, z_send, z_recv,
    ag_send, ag_recv, rs_send, rs_recv, q_send, q_recv, o_send, o_recv, s_send, s_recv, r_send, r_recv,
):
    z = lax.axis_index("sp")
    tp = lax.axis_index("tp")
    x, c = tp // CORES, tp % CORES
    half = x % 2
    idx = half * CORES + c
    group = tp - idx
    gsize = nx * CORES // KVH
    src_rows = src_v.shape[0]
    tgt_rows = tgt_v.shape[0]
    sub_rows = src_rows // 2
    block = kvb.shape[3]
    hops = nz // 2
    width = nx * tgt_rows
    scale2 = HEAD ** -0.5 * math.log2(math.e)

    def chip(k):
        return lax.rem(x + k + nx, nx)

    def same_core(k):
        return {"tp": chip(k) * CORES + c}

    partner = {"tp": tp + 1 - 2 * c}
    across = {"tp": (x + 1 - 2 * half) * CORES + c}

    def zpos(k):
        return lax.rem(z + k + nz, nz)

    def remote(src, dst, ss, rs, dev):
        return pltpu.make_async_remote_copy(
            src_ref=src, dst_ref=dst, send_sem=ss, recv_sem=rs, device_id=dev, device_id_type=MESH
        )

    loads = [
        (src_hbm, src_v), (kv1_hbm, kvin.at[0]), (kv2_hbm, kvin.at[1]), (tgt_hbm, tgt_v),
        (q1_hbm, wq.at[0, c]), (o1_hbm, wo.at[0, c]), (wg_hbm, wgv.at[0, c]), (wv_hbm, wgv.at[1, c]),
        (wd_hbm, wdn.at[c]), (taps_hbm, taps.at[c]), (q2_hbm, wq.at[1, c]), (o2_hbm, wo.at[1, c]),
    ]
    local = [pltpu.make_async_copy(a, b, loc_sem.at[i]) for i, (a, b) in enumerate(loads)]
    for cp in local:
        cp.start()

    barrier = pltpu.get_barrier_semaphore()
    peers = [same_core(k) for k in range(1, nx)]
    peers += [{"tp": group + lax.rem(idx + r, gsize)} for r in range(1, gsize)]
    peers += [{"sp": zpos(1)}, {"sp": zpos(-1)}, {"sp": zpos(2 * c - 1), "tp": tp + 1 - 2 * c}]
    for dev in peers:
        pl.semaphore_signal(barrier, inc=1, device_id=dev, device_id_type=MESH)

    local[0].wait()
    rows = normed(src_v[...].astype(F32), sgain[...]).astype(BF16)
    rows_x[x, 0] = rows[:sub_rows]
    rows_x[x, 1] = rows[sub_rows:]
    local[1].wait()
    local[2].wait()
    w2[c] = jnp.concatenate([kvin[0], kvin[1]], axis=1)
    local[3].wait()
    hb[0, x] = normed(tgt_v[...].astype(F32), pre1[...]).astype(BF16)
    pl.semaphore_wait(barrier, len(peers))

    def x_copy(d, h, s, origin):
        ref = rows_x.at[origin, s]
        return remote(ref, ref, x_send.at[d, h, s], x_recv.at[d, h, s], same_core(1 - 2 * d))

    for s in range(2):
        for d in range(2):
            x_copy(d, 0, s, x).start()

    weights = [
        (w2.at[c], w2.at[c]), (q1_hbm, wq.at[0, c]), (o1_hbm, wo.at[0, c]), (wg_hbm, wgv.at[0, c]),
        (wv_hbm, wgv.at[1, c]), (wd_hbm, wdn.at[c]), (taps_hbm, taps.at[c]), (q2_hbm, wq.at[1, c]),
        (o2_hbm, wo.at[1, c]),
    ]
    w_copies = [remote(a, b, w_send.at[i], w_recv.at[i], partner) for i, (a, b) in enumerate(weights)]
    w_copies[0].start()

    def project(chunk):
        left = dot(chunk, w2[0])
        right = dot(chunk, w2[1])
        w = HEAD // 2
        return [
            jnp.concatenate([left[:, l * w : (l + 1) * w], right[:, l * w : (l + 1) * w]], axis=1).astype(BF16)
            for l in range(2)
        ]

    def place(outs, origin, at):
        per = nx // 2
        for l in range(2):
            kv_st[origin // per, l, pl.ds(pl.multiple_of(lax.rem(origin, per) * src_rows, src_rows), src_rows), :] = (
                outs[l][at : at + src_rows]
            )

    def two_subs(origin):
        return [rows_x[origin, 0], rows_x[origin, 1]]

    w_copies[0].wait_recv()
    place(project(jnp.concatenate(two_subs(x), axis=0)), x, 0)

    far = nx // 2

    def x_hop(h, last):
        right_o, left_o = chip(-h), chip(h)
        for s in range(2):
            x_copy(0, h - 1, s, right_o).wait_recv()
            if not last or s == 0:
                x_copy(0, h, s, right_o).start()
            x_copy(1, h - 1, s, left_o).wait_recv()
            if not last or s == 1:
                x_copy(1, h, s, left_o).start()
        outs = project(jnp.concatenate(two_subs(right_o) + two_subs(left_o), axis=0))
        place(outs, right_o, 0)
        place(outs, left_o, src_rows)

    for h in range(1, far):
        x_hop(h, h == far - 1)
        for cp in w_copies[3 * h - 2 : 3 * h + 1]:
            cp.start()
    for cp in w_copies[3 * far - 2 :]:
        cp.start()
    x_copy(0, far - 1, 0, chip(far)).wait_recv()
    x_copy(1, far - 1, 1, chip(far)).wait_recv()
    place(project(jnp.concatenate(two_subs(chip(far)), axis=0)), chip(far), 0)

    e_copies = [
        remote(kv_st.at[1 - half, l], kvb.at[l, z, half], e_send.at[l], e_recv.at[l], across) for l in range(2)
    ]
    for cp in e_copies:
        cp.start()
    for l in range(2):
        kvb[l, z, half] = kv_st[half, l]

    order = sorted(range(1, nx), key=lambda k: -min(k, nx - k))

    def ag_copy(ph, k):
        return remote(hb.at[ph, x], hb.at[ph, x], ag_send.at[ph, k], ag_recv.at[ph, k], same_core(k))

    def ag_start(ph):
        for k in order:
            ag_copy(ph, k).start()

    def ag_wait(ph):
        for k in order:
            ref = hb.at[ph, chip(-k)]
            remote(ref, ref, ag_send.at[ph, k], ag_recv.at[ph, k], same_core(k)).wait_recv()
        return hb[ph].astype(F32).reshape(width, -1).astype(BF16)

    def rs_copy(ph, k):
        return remote(sb.at[ph, chip(k)], rb.at[ph, x], rs_send.at[ph, k], rs_recv.at[ph, k], same_core(k))

    def rs_start(ph, total):
        sb[ph] = total.reshape(nx, tgt_rows, -1).astype(BF16)
        for k in order:
            rs_copy(ph, k).start()
        rb[ph, x] = sb[ph, x]

    def rs_wait(ph):
        for k in order:
            remote(sb.at[ph, chip(k)], rb.at[ph, chip(-k)], rs_send.at[ph, k], rs_recv.at[ph, k], same_core(k)).wait_recv()
        return jnp.sum(rb[ph].astype(F32), axis=0)

    piece = block // 2

    def z_copy(l, d, h, s, origin):
        kind = lax.rem(half + s // 2, 2)
        ref = kvb.at[l, origin, kind, pl.ds((s % 2) * piece, piece)]
        return remote(ref, ref, z_send.at[l, d, h, s], z_recv.at[l, d, h, s], {"sp": zpos(1 - 2 * d)})

    def z_start(l, s):
        for d in range(2):
            z_copy(l, d, 0, s, z).start()

    def z_hop(l, h, last):
        right_o, left_o = zpos(-h), zpos(h)
        for s in range(SUBS):
            for d, origin in ((0, right_o), (1, left_o)):
                z_copy(l, d, h - 1, s, origin).wait_recv()
                if not last or s // 2 == d:
                    z_copy(l, d, h, s, origin).start()

    def z_last(l):
        for s in range(SUBS):
            z_copy(l, s // 2, hops - 1, s, zpos(hops)).wait_recv()

    z_start(0, 0)
    z_start(0, 1)
    ag_start(0)
    e_copies[0].wait_recv()
    z_start(0, 2)
    z_start(0, 3)
    e_copies[1].wait_recv()

    def q_slot(l, i):
        return qb.at[l, i]

    def q_copy(l, r):
        return remote(
            qb.at[l, idx], qb.at[l, idx], q_send.at[l, r], q_recv.at[l, r], {"tp": group + lax.rem(idx + r, gsize)}
        )

    def q_project(l, hidden):
        for hh in range(CORES):
            qb[l, idx, hh * width : (hh + 1) * width, :] = dot(hidden, wq[l, hh]).astype(BF16)
        for r in range(1, gsize):
            q_copy(l, r).start()

    def q_wait(l):
        for r in range(1, gsize):
            ref = qb.at[l, lax.rem(idx + gsize - r, gsize)]
            remote(ref, ref, q_send.at[l, r], q_recv.at[l, r], {"tp": group}).wait_recv()
        m_run[...] = jnp.full_like(m_run, -jnp.inf)
        l_run[...] = jnp.zeros_like(l_run)
        acc[...] = jnp.zeros_like(acc)

    def absorb(l, keys, values):
        queries = qb[l].reshape(gsize * CORES * width, HEAD)
        scores = dot(keys, queries, ((1,), (1,)))
        m_old = m_run[...]
        m_new = jnp.maximum(m_old, jnp.max(scores, axis=0, keepdims=True))
        rescale = jnp.exp2((m_old - m_new) * scale2)
        weights = jnp.exp2((scores - m_new) * scale2)
        l_run[...] = l_run[...] * rescale + jnp.sum(weights, axis=0, keepdims=True)
        acc[...] = acc[...] * rescale + dot(values, weights.astype(BF16), ((0,), (0,)))
        m_run[...] = m_new

    def absorb_pair(l, a, b):
        absorb(
            l,
            jnp.concatenate([kvb[l, a, 0], kvb[l, b, 0]], axis=0),
            jnp.concatenate([kvb[l, a, 1], kvb[l, b, 1]], axis=0),
        )

    def o_copies(l, r):
        to = lax.rem(idx + r, gsize)
        dev = {"tp": group + to}
        return [
            remote(o_st.at[l, to], ob.at[l, idx], o_send.at[l, r], o_recv.at[l, r], dev),
            remote(s_st.at[l, to], st.at[l, idx], s_send.at[l, r], s_recv.at[l, r], dev),
        ]

    def o_start(l):
        total = l_run[...]
        share = (acc[...] / total).astype(BF16)
        cols = CORES * width
        for i in range(gsize):
            at = slice(i * cols, (i + 1) * cols)
            o_st[l, i] = share[:, at]
            s_st[l, i] = jnp.concatenate(
                [m_run[:, at], total[:, at], jnp.zeros((6, cols), F32)], axis=0
            )
        for r in range(1, gsize):
            for cp in o_copies(l, r):
                cp.start()
        ob[l, idx] = o_st[l, idx]
        st[l, idx] = s_st[l, idx]

    def o_wait(l):
        for r in range(1, gsize):
            at = lax.rem(idx + gsize - r, gsize)
            remote(o_st.at[l, at], ob.at[l, at], o_send.at[l, r], o_recv.at[l, r], {"tp": group}).wait_recv()
            remote(s_st.at[l, at], st.at[l, at], s_send.at[l, r], s_recv.at[l, r], {"tp": group}).wait_recv()
        maxima = [st[l, i, 0:1, :] for i in range(gsize)]
        top = functools.reduce(jnp.maximum, maxima)
        shares = [st[l, i, 1:2, :] * jnp.exp2((maxima[i] - top) * scale2) for i in range(gsize)]
        whole = functools.reduce(jnp.add, shares)
        mixed = functools.reduce(jnp.add, [ob[l, i].astype(F32) * shares[i] for i in range(gsize)])
        heads = (mixed / whole).T.astype(BF16)
        return sum(dot(heads[hh * width : (hh + 1) * width], wo[l, hh]) for hh in range(CORES))

    for h in range(1, 3):
        z_hop(0, h, False)
    hidden = ag_wait(0)
    local[4].wait()
    w_copies[1].wait_recv()
    q_project(0, hidden)
    z_hop(0, 3, False)
    q_wait(0)
    absorb(0, kvb[0, z, 0], kvb[0, z, 1])

    def early(h, carry):
        absorb_pair(0, zpos(-h), zpos(h))
        return carry

    lax.fori_loop(1, 3, early, 0)

    def body(h, carry):
        z_hop(0, h, False)
        absorb_pair(0, zpos(1 - h), zpos(h - 1))
        return carry

    lax.fori_loop(4, hops - 1, body, 0)
    z_hop(0, hops - 1, True)
    for s in range(SUBS):
        z_start(1, s)
    absorb_pair(0, zpos(2 - hops), zpos(hops - 2))
    absorb_pair(0, zpos(1 - hops), zpos(hops - 1))
    z_last(0)
    absorb(0, kvb[0, zpos(hops), 0], kvb[0, zpos(hops), 1])

    o_start(0)
    z_hop(1, 1, False)
    local[5].wait()
    w_copies[2].wait_recv()
    rs_start(0, o_wait(0))
    z_hop(1, 2, False)
    after_first = tgt_v[...].astype(F32) + normed(rs_wait(0), post1[...])
    hb[1, x] = normed(after_first, fpre[...]).astype(BF16)
    ag_start(1)
    resid[...] = after_first
    z_hop(1, 3, False)
    for i in (6, 7, 8, 9):
        local[i].wait()
    for i in (3, 4, 5, 6):
        w_copies[i].wait_recv()
    hidden = ag_wait(1)
    units = wdn.shape[1]
    span = up.shape[2] // 4
    for kind in range(2):
        for core in range(CORES):
            at = (kind * CORES + core) * span
            up[:, :, at : at + units] = dot(hidden, wgv[kind, core]).reshape(nx, tgt_rows, units).astype(BF16)
    rim_a = remote(up.at[pl.ds(0, nx - 1)], rim.at[pl.ds(c, nx - 1)], r_send.at[0], r_recv.at[0], partner)
    rim_a.start()
    last_slot = (nx - 1) * (1 - c)
    rim_b = remote(
        up.at[nx - 1], rim.at[last_slot], r_send.at[1], r_recv.at[1], {"sp": zpos(c), "tp": tp + 1 - 2 * c}
    )
    sends_b = jnp.logical_or(c == 0, z < nz - 1)
    gets_b = jnp.logical_or(c == 1, z > 0)

    @pl.when(sends_b)
    def _():
        rim_b.start()

    @pl.when(jnp.logical_not(gets_b))
    def _():
        rim[0] = jnp.zeros(rim.shape[1:], rim.dtype)

    z_hop(1, 4, False)
    rim_a.wait_recv()

    @pl.when(gets_b)
    def _():
        rim_b.wait_recv()

    def conv(kind, core):
        at = (kind * CORES + core) * span
        here = up[:, :, at : at + units].astype(F32)
        before = rim[:, :, at : at + units].astype(F32)
        t = taps[core][3 * kind : 3 * kind + 3, :units]
        one = jnp.concatenate([before[:, -1:], here[:, :-1]], axis=1)
        two = jnp.concatenate([before[:, -2:], here[:, :-2]], axis=1)
        return t[0:1] * two + t[1:2] * one + t[2:3] * here

    total = 0.0
    for core in range(CORES):
        gated = jax.nn.gelu(conv(0, core), approximate=True) * conv(1, core)
        total += dot(gated.reshape(width, units).astype(BF16), wdn[core])
    rs_start(1, total)
    z_hop(1, 5, False)
    after_ffn = resid[...] + normed(rs_wait(1), fpost[...])
    hb[2, x] = normed(after_ffn, pre2[...]).astype(BF16)
    ag_start(2)
    resid[...] = after_ffn
    z_hop(1, 6, False)
    hidden = ag_wait(2)
    local[10].wait()
    w_copies[7].wait_recv()
    q_project(1, hidden)
    z_hop(1, 7, True)
    z_last(1)
    q_wait(1)
    together = 4

    def chunk(i, carry):
        part = kvb[1, pl.ds(i * together, together)]
        absorb(1, part[:, 0].reshape(together * block, HEAD), part[:, 1].reshape(together * block, HEAD))
        return carry

    lax.fori_loop(0, nz // together, chunk, 0)
    o_start(1)
    local[11].wait()
    w_copies[8].wait_recv()
    rs_start(2, o_wait(1))
    out_ref[...] = resid[...] + normed(rs_wait(2), post2[...])

    for h in range(far):
        for s in range(2):
            for d in range(2):
                if h < far - 1 or s == d:
                    x_copy(d, h, s, x).wait_send()
    for cp in w_copies + e_copies:
        cp.wait_send()
    for l in range(2):

        def drained(h, carry):
            for s in range(SUBS):
                for d in range(2):
                    z_copy(l, d, h, s, z).wait_send()
            return carry

        lax.fori_loop(0, hops - 1, drained, 0)
        for s in range(SUBS):
            z_copy(l, s // 2, hops - 1, s, z).wait_send()
        for r in range(1, gsize):
            q_copy(l, r).wait_send()
            for cp in o_copies(l, r):
                cp.wait_send()
    for ph in range(3):
        for k in order:
            ag_copy(ph, k).wait_send()
            rs_copy(ph, k).wait_send()
    rim_a.wait_send()

    @pl.when(sends_b)
    def _():
        rim_b.wait_send()


def solution(mesh):
    nx, nz = mesh.shape["tp"] // CORES, mesh.shape["sp"]
    gsize = nx * CORES // KVH

    def per_device(
        target, source, source_gain, pre_first, query_first, keyval_first, out_first, post_first, ffn_pre,
        w_gate, w_value, conv_gate, conv_value, w_down, ffn_post, pre_second, query_second, keyval_second,
        out_second, post_second,
    ):
        depth = target.shape[1]
        tgt_rows, src_rows = target.shape[0], source.shape[0]
        units = w_gate.shape[1]
        kvw = keyval_first.shape[1]
        width = nx * tgt_rows
        block = nx // 2 * src_rows
        hops = nz // 2
        lanes = -(-units // HEAD) * HEAD
        taps = jnp.pad(jnp.concatenate([conv_gate, conv_value], axis=0), ((0, 2), (0, lanes - units)))
        vmem = pl.BlockSpec(memory_space=pltpu.VMEM)
        anyw = pl.BlockSpec(memory_space=pl.ANY)
        dma = pltpu.SemaphoreType.DMA
        cols = CORES * width
        gains = [g.reshape(1, depth) for g in (source_gain, pre_first, post_first, ffn_pre, ffn_post, pre_second, post_second)]
        return pl.pallas_call(
            functools.partial(kernel, nx, nz),
            out_shape=jax.ShapeDtypeStruct((tgt_rows, depth), F32),
            in_specs=[anyw] * 3 + [vmem] * 7 + [anyw] * 9,
            out_specs=vmem,
            scratch_shapes=[
                pltpu.VMEM((src_rows, depth), BF16),
                pltpu.VMEM((tgt_rows, depth), BF16),
                pltpu.VMEM((2, depth, kvw), BF16),
                pltpu.VMEM((CORES, depth, 2 * kvw), BF16),
                pltpu.VMEM((2, CORES, depth, HEAD), BF16),
                pltpu.VMEM((2, CORES, HEAD, depth), BF16),
                pltpu.VMEM((2, CORES, depth, units), BF16),
                pltpu.VMEM((CORES, units, depth), BF16),
                pltpu.VMEM((CORES, 8, lanes), F32),
                pltpu.VMEM((nx, 2, src_rows // 2, depth), BF16),
                pltpu.VMEM((2, 2, block, HEAD), BF16),
                pltpu.VMEM((2, nz, 2, block, HEAD), BF16),
                pltpu.VMEM((3, nx, tgt_rows, depth), BF16),
                pltpu.VMEM((3, nx, tgt_rows, depth), BF16),
                pltpu.VMEM((3, nx, tgt_rows, depth), BF16),
                pltpu.VMEM((2, gsize, cols, HEAD), BF16),
                pltpu.VMEM((2, gsize, HEAD, cols), BF16),
                pltpu.VMEM((2, gsize, HEAD, cols), BF16),
                pltpu.VMEM((2, gsize, 8, cols), F32),
                pltpu.VMEM((2, gsize, 8, cols), F32),
                pltpu.VMEM((HEAD, gsize * cols), F32),
                pltpu.VMEM((1, gsize * cols), F32),
                pltpu.VMEM((1, gsize * cols), F32),
                pltpu.VMEM((nx, tgt_rows, 4 * lanes), BF16),
                pltpu.VMEM((nx, tgt_rows, 4 * lanes), BF16),
                pltpu.VMEM((tgt_rows, depth), F32),
                dma((12,)),
                dma((9,)), dma((9,)),
                dma((2, nx // 2, 2)), dma((2, nx // 2, 2)),
                dma((2,)), dma((2,)),
                dma((2, 2, hops, SUBS)), dma((2, 2, hops, SUBS)),
                dma((3, nx)), dma((3, nx)),
                dma((3, nx)), dma((3, nx)),
                dma((2, gsize)), dma((2, gsize)),
                dma((2, gsize)), dma((2, gsize)),
                dma((2, gsize)), dma((2, gsize)),
                dma((2,)), dma((2,)),
            ],
            compiler_params=pltpu.CompilerParams(
                collective_id=0, has_side_effects=True, vmem_limit_bytes=56 * 1024 * 1024
            ),
        )(
            target, source, taps, *gains, query_first, query_second, keyval_first, keyval_second,
            out_first, out_second, w_gate, w_value, w_down,
        )

    placed = (
        P(("grp", "sp", "tp"), None), P(("grp", "sp", "tp"), None), P(), P(), P(None, "tp"), P(None, "tp"),
        P("tp", None), P(), P(), P(None, "tp"), P(None, "tp"), P(None, "tp"), P(None, "tp"), P("tp", None),
        P(), P(), P(None, "tp"), P(None, "tp"), P("tp", None), P(),
    )
    return jax.shard_map(
        per_device, mesh=mesh, in_specs=placed, out_specs=P(("grp", "sp", "tp"), None), check_vma=False
    )
```

time: 382 us -> 179 us (0.47)
  Pallas kernels: 0 us -> 170 us
  waiting for transfers between devices: 167 us -> 0 us
  blocking collectives: 97.2 us -> 0 us
  starting transfers between devices: 70 us -> 0 us
  matrix products: 16.9 us -> 0 us
  between operations: 13.8 us -> 0.02 us
  other arithmetic: 12.8 us -> 0.61 us
  local copies, waits for them, and re-layouts: 3.23 us -> 7.79 us
    pallas_call x0 -> x1, Pallas kernels: none -> 170 us  [per_device(): pl.pallas_call(functools.partial(kernel, nx, nz), out_shape=jax.ShapeDtyp...]
    all_gather x3 -> x0, waiting for transfers between devices: 125 us -> none  [the longest x1 83.2 us: key_columns(): lax.all_gather(source_rows, 'tp', axis=0, tiled=True)]
    ppermute x20 -> x0, starting transfers between devices: 63.3 us -> none  [the longest x18 57.9 us: swapped(): return lax.ppermute(block, axis, route)]
    all_gather x3 -> x0, blocking collectives: 50.6 us -> none  [project_rows(): shard_rows = lax.all_gather(rows_here, 'tp', axis=0, tiled=True)]
    all_to_all x2 -> x0, blocking collectives: 46.6 us -> none  [sent_and_summed(): lax.all_to_all(parts, axis, split_axis=0, concat_axis=0, tiled=True)]
    ppermute x20 -> x0, waiting for transfers between devices: 27.6 us -> none  [the longest x18 26.6 us: swapped(): return lax.ppermute(block, axis, route)]
    dot_general x12 -> x0, matrix products: 16.9 us -> none  [the longest x2 5.49 us: absorber(): jnp.einsum('thd,ds->ths', query_heads, key_block, preferred_element_type=...]
    all_to_all x1 -> x0, waiting for transfers between devices: 13.9 us -> none  [sent_and_summed(): lax.all_to_all(parts, axis, split_axis=0, concat_axis=0, tiled=True)]
  transfers between devices with their start and end apart: 24 -> 0, of which waited for: 16 -> 0; matrix products, arithmetic and copies ran while one was open for 2% -> 0% of each run, Pallas kernels for 0% -> 0%
where the time goes in v1:
time: 179 us
  Pallas kernels  170 us (95%)
  local copies, waits for them, and re-layouts  7.79 us (4%)
    pallas_call x1, Pallas kernels, per_device(): pl.pallas_call(functools.partial(kernel, nx, nz), out_shape=jax.ShapeDtyp...  170 us
    unnamed x15, local copies, waits for them, and re-layouts  7.79 us

profile of v1, /device:TPU:65, one launch (start us, length us, event | category | flops | bytes accessed | tf_op | source)
XLA Modules:
  0.0 178.8 jit_solution(2700780422243922774)
XLA Ops:
  0.0 0.0 copy-start.4
  0.0 0.0 copy-start.3
  0.0 0.7 copy-done.4
  0.7 0.0 copy-done.3
  0.7 0.0 copy-start.2
  0.7 0.6 select_maximum_fusion.taps_hbm
  1.3 0.0 copy-start
  1.3 2.0 %copy.21.kv1_hbm = bf16[2048,64]{1,0:T(8,128)(2,1)} copy(bf16[2048,64]{0,1:T(8,128)(2,1)} %param.25) | data formatting | bytes 524288 | tf_op args[5]
  3.3 0.0 copy-done.2
  3.3 1.0 copy.22.kv2_hbm
  4.4 0.0 copy-done
  4.4 0.0 copy-start.1
  4.4 1.3 copy.23.wg_hbm
  5.6 0.0 copy-done.1
  5.6 1.3 copy.24.wv_hbm
  6.9 170.4 %shard_map.190 = f32[8,2048]{1,0:T(8,128)} custom-call(bf16[8,2048]{1,0:T(8,128)(2,1)} %tgt_hbm.1, bf16[64,2048]{1,0:T(8,128)(2,1)} %src_hbm.1, f32[8,256]{1,0:T(8,128)} %select_maximum_fusion.taps_hbm, f32[1,2048]{1,0:T(1,128)} %bitcast.7, f32[1,2048]{1,0:T(1,128)} %bitcast.8, f32[1,2048]{1,0:T(1,128)} %bitcast.9, f32[1,2048]{1,0:T(1,128)} %bitcast.10, ...), custom_call_target="tpu_custom_call" | custom-call | tf_op jit(solution)/shard_map/pallas_call | solution.py:478
  177.3 1.5 copy.26
Async XLA Ops:
  0.0 0.7 copy-start.4
  0.0 0.7 copy-start.3
  0.7 2.6 %copy-start.2 = (bf16[2048,64]{0,1:T(8,128)(2,1)S(1)}, bf16[2048,64]{0,1:T(8,128)(2,1)}, u32[]{:S(2)}) copy-start(bf16[2048,64]{0,1:T(8,128)(2,1)} %param.37) | copy-start | bytes 786436
  1.3 3.0 %copy-start = (bf16[2048,176]{0,1:T(8,128)(2,1)S(1)}, bf16[2048,176]{0,1:T(8,128)(2,1)}, u32[]{:S(2)}) copy-start(bf16[2048,176]{0,1:T(8,128)(2,1)} %param.29) | copy-start | bytes 2162692
  4.4 1.3 copy-start.1
